TPU v7x, 32 devices: a whole 2x2x4 slice. The times are simulated.
32 devices in a mesh: grp: 2 (over y), sp: 4 (over z), tp: 4 (over x, core).
Axes of the slice: x: 2, y: 2, z: 4, core: 2. Of those that a mesh axis runs over, the one named last changes fastest.
Arguments:
- tokens: bfloat16 [3072, 4096], P(('grp', 'sp'), 'tp'), parts along dimension 0, may hold values from -6 to 6
- proj_b: bfloat16 [2, 4096, 2048], P(None, 'sp', 'tp'), may hold values from -0.09375 to 0.09375
- proj_c: bfloat16 [2, 4096, 2048], P(None, 'sp', 'tp'), may hold values from -0.09375 to 0.09375
- proj_x: bfloat16 [2, 4096, 2048], P(None, 'sp', 'tp'), may hold values from -0.09375 to 0.09375
- proj_out: bfloat16 [2, 2048, 4096], P(None, 'sp', 'tp'), may hold values from -1 to 1
- conv_taps: float32 [2, 3, 2048], P(None, None, 'tp'), may hold values from -3 to 3
- ln_gain: float32 [2, 4096], P(None, 'tp'), may hold values from 0.1 to 1.9
- ln_bias: float32 [2, 4096], P(None, 'tp'), may hold values from -2 to 2
Outputs:
- result: bfloat16 [3072, 4096], P(('grp', 'sp'), 'tp'), parts along dimension 0
There are 2 independent parts, one for each index of `grp`. A program takes and returns all parts, laid end to end along the dimension named above; an argument that names none is the same for every part. Nothing has to cross between parts.
All inputs are finite; a program needn't handle non-finite values.
Results may differ from a plain program's by a relative error of at most 0.012.
Values may be sent and summed in bfloat16 or wider, within the bound.
A program may use at most 128 MiB of HBM per device.

v0:
```python
import jax
import jax.numpy as jnp
from jax import lax
from jax.sharding import PartitionSpec as P

LAYERS = 2
norm_eps = 1e-05


def from_behind(block, axis, distance):
    devices = range(lax.axis_size(axis))
    route = [(i - distance, i) for i in devices if i - distance in devices]
    return lax.ppermute(block, axis, route)


def local(tokens, proj_b, proj_c, proj_x, proj_out, conv_taps, ln_gain, ln_bias):
    residual_scale = (2.0 * LAYERS) ** 0.25
    hidden = tokens
    whole_b, whole_c, whole_x, whole_out = (
        lax.all_gather(proj_b, "sp", axis=1, tiled=True),
        lax.all_gather(proj_c, "sp", axis=1, tiled=True),
        lax.all_gather(proj_x, "sp", axis=1, tiled=True),
        lax.all_gather(proj_out, "sp", axis=1, tiled=True),
    )
    for layer_index in range(LAYERS):
        gathered = lax.all_gather(hidden, "tp", axis=1, tiled=True)
        count_rows = gathered.shape[0]
        acc_b = jnp.dot(gathered, whole_b[layer_index], preferred_element_type=jnp.float32)
        acc_c = jnp.dot(gathered, whole_c[layer_index], preferred_element_type=jnp.float32)
        acc_x = jnp.dot(gathered, whole_x[layer_index], preferred_element_type=jnp.float32)
        out_gate = lax.optimization_barrier(acc_b.astype(jnp.bfloat16))
        in_gate = lax.optimization_barrier(acc_c.astype(jnp.bfloat16))
        values = lax.optimization_barrier(acc_x.astype(jnp.bfloat16))
        gated_in = in_gate.astype(jnp.float32) * values.astype(jnp.float32)
        reach = conv_taps.shape[1] - 1
        fringe = from_behind(gated_in[count_rows - reach :], "sp", 1)
        padded = jnp.concatenate([fringe, gated_in], 0)
        conv_out = jnp.zeros_like(gated_in)
        for tap_index in range(reach + 1):
            conv_out = (
                conv_out
                + conv_taps[layer_index, tap_index] * padded[tap_index : tap_index + count_rows]
            )
        branch = (out_gate.astype(jnp.float32) * conv_out).astype(jnp.bfloat16)
        all_branch = lax.all_gather(branch, "tp", axis=1, tiled=True)
        acc_out = jnp.dot(all_branch, whole_out[layer_index], preferred_element_type=jnp.float32)
        mixed = lax.optimization_barrier(acc_out.astype(jnp.bfloat16))
        summed = residual_scale * hidden.astype(jnp.float32) + mixed.astype(jnp.float32)
        width_all = summed.shape[1] * lax.axis_size("tp")
        mean = (lax.psum(jnp.sum(summed, axis=1), "tp") / width_all)[:, None]
        centered = summed - mean
        variance = (lax.psum(jnp.sum(centered * centered, axis=1), "tp") / width_all)[:, None]
        hidden = (
            centered * lax.rsqrt(variance + norm_eps) * ln_gain[layer_index] + ln_bias[layer_index]
        ).astype(jnp.bfloat16)
    return hidden


def solution(mesh):
    return jax.shard_map(
        local,
        mesh=mesh,
        in_specs=(
            P(("grp", "sp"), "tp"),
            P(None, "sp", "tp"),
            P(None, "sp", "tp"),
            P(None, "sp", "tp"),
            P(None, "sp", "tp"),
            P(None, None, "tp"),
            P(None, "tp"),
            P(None, "tp"),
        ),
        out_specs=P(("grp", "sp"), "tp"),
        check_vma=False,
    )
```

profile of v0, /device:TPU:0, one launch (start us, length us, event | category | flops | bytes accessed | tf_op | source)
XLA Modules:
  0.0 767.4 jit_solution(15799623841625418125)
XLA Ops:
  10.0 30.2 %all-gather.9.cloned.1.call-done = bf16[384,4096]{1,0:T(8,128)(2,1)} async-done(((bf16[384,1024]{1,0:T(8,128)(2,1)}), bf16[384,4096]{1,0:T(8,128)(2,1)}) %all-gather.9.cloned.1.call-update) | async-done | bytes 3145744 | tf_op jit(solution)/shard_map/all_gather | solution.py:26
  40.2 151.2 %all-gather.13.cloned.1.call-done = bf16[2,4096,512]{2,1,0:T(8,128)(2,1)} async-done(((bf16[2,1024,512]{2,1,0:T(8,128)(2,1)}), bf16[2,4096,512]{2,1,0:T(8,128)(2,1)}) %all-gather.13.cloned.1.call-update) | async-done | bytes 8388624 | tf_op jit(solution)/shard_map/all_gather | solution.py:21
  191.4 4.9 fusion.11
  196.3 144.5 %all-gather.15.cloned.1.call-done = bf16[2,4096,512]{2,1,0:T(8,128)(2,1)} async-done(((bf16[2,1024,512]{2,1,0:T(8,128)(2,1)}), bf16[2,4096,512]{2,1,0:T(8,128)(2,1)}) %all-gather.15.cloned.1.call-update) | async-done | bytes 8388624 | tf_op jit(solution)/shard_map/all_gather | solution.py:22
  340.8 4.9 fusion.12
  345.8 1.3 collective-permute-start
  347.1 142.9 %all-gather.11.cloned.1.call-done = bf16[2,4096,512]{2,1,0:T(8,128)(2,1)} async-done(((bf16[2,1024,512]{2,1,0:T(8,128)(2,1)}), bf16[2,4096,512]{2,1,0:T(8,128)(2,1)}) %all-gather.11.cloned.1.call-update) | async-done | bytes 8388624 | tf_op jit(solution)/shard_map/all_gather | solution.py:20
  490.0 4.9 fusion.10
  496.2 143.1 %all-gather.19.cloned.1.call-done = bf16[2,2048,1024]{2,1,0:T(8,128)(2,1)} async-done(((bf16[2,512,1024]{2,1,0:T(8,128)(2,1)}), bf16[2,2048,1024]{2,1,0:T(8,128)(2,1)}) %all-gather.19.cloned.1.call-update) | async-done | bytes 8388624 | tf_op jit(solution)/shard_map/all_gather | solution.py:23
  639.3 19.3 %all-gather.17.cloned.1.call-done = bf16[384,2048]{1,0:T(8,128)(2,1)} async-done(((bf16[384,512]{1,0:T(8,128)(2,1)}), bf16[384,2048]{1,0:T(8,128)(2,1)}) %all-gather.17.cloned.1.call-update) | async-done | bytes 1572880 | tf_op jit(solution)/shard_map/all_gather | solution.py:45
  658.6 4.5 fusion.8
  663.4 5.9 psum.28
  669.7 5.7 psum.29
  675.3 1.3 add_convert_fusion.1
  676.8 29.9 %all-gather.21.cloned.1.call-done = bf16[384,4096]{1,0:T(8,128)(2,1)} async-done(((bf16[384,1024]{1,0:T(8,128)(2,1)}), bf16[384,4096]{1,0:T(8,128)(2,1)}) %all-gather.21.cloned.1.call-update) | async-done | bytes 3145744 | tf_op jit(solution)/shard_map/all_gather | solution.py:26
  706.7 5.1 fusion.14
  711.8 4.1 fusion.15
  716.0 3.6 collective-permute-start.1
  719.6 1.8 fusion.13
  722.5 19.9 %all-gather.23.cloned.1.call-done = bf16[384,2048]{1,0:T(8,128)(2,1)} async-done(((bf16[384,512]{1,0:T(8,128)(2,1)}), bf16[384,2048]{1,0:T(8,128)(2,1)}) %all-gather.23.cloned.1.call-update) | async-done | bytes 1572880 | tf_op jit(solution)/shard_map/all_gather | solution.py:45
  742.4 4.5 fusion.9
  747.2 5.9 psum.30
  753.5 5.7 psum.31
  759.2 1.3 add_convert_fusion
  (52 shorter events, 7.4 us)
Async XLA Ops:
  6.5 33.6 %all-gather.9.cloned.1.call-start = ((), (), s32[]{:S(2)}) async-start(), calls=%async_computation | async-start | bytes 3932160 | tf_op jit(solution)/shard_map/all_gather | solution.py:26
  7.3 184.1 %all-gather.13.cloned.1.call-start = ((), (), s32[]{:S(2)}) async-start(), calls=%async_computation.2 | async-start | bytes 10485760 | tf_op jit(solution)/shard_map/all_gather | solution.py:21
  8.0 332.8 %all-gather.15.cloned.1.call-start = ((), (), s32[]{:S(2)}) async-start(), calls=%async_computation.3 | async-start | bytes 10485760 | tf_op jit(solution)/shard_map/all_gather | solution.py:22
  8.7 1.2 copy-start.2
  8.8 481.3 %all-gather.11.cloned.1.call-start = ((), (), s32[]{:S(2)}) async-start(), calls=%async_computation.1 | async-start | bytes 10485760 | tf_op jit(solution)/shard_map/all_gather | solution.py:20
  9.3 630.0 %all-gather.19.cloned.1.call-start = ((), (), s32[]{:S(2)}) async-start(), calls=%async_computation.5 | async-start | bytes 10485760 | tf_op jit(solution)/shard_map/all_gather | solution.py:23
  9.9 648.6 %all-gather.17.cloned.1.call-start = ((), (), s32[]{:S(2)}) async-start(), calls=%async_computation.4 | async-start | bytes 1966080 | tf_op jit(solution)/shard_map/all_gather | solution.py:45
  345.8 149.2 %collective-permute-start = (f32[2,512]{1,0:T(2,128)S(1)}, f32[2,512]{1,0:T(2,128)S(1)}, u32[]{:S(2)}, u32[]{:S(2)}) collective-permute-start(f32[2,512]{1,0:T(2,128)S(1)} %slice.99), channel_id=1, source_target_pairs={{0,4},{4,8},{8,12},{1,5},{5,9},{9,13},{2,6},{6,10},{10,14},{3,7},{... | collective-permute-start | bytes 12296 | tf_op jit(solution)/shard_map/ppermute | solution.py:13
  495.0 1.2 copy-start.3
  495.0 1.2 copy-start.4
  496.1 210.6 %all-gather.21.cloned.1.call-start = ((), (), s32[]{:S(2)}) async-start(), calls=%async_computation.6 | async-start | bytes 3932160 | tf_op jit(solution)/shard_map/all_gather | solution.py:26
  496.2 166.8 %copy-start.1 = (bf16[384,1024]{1,0:T(8,128)(2,1)S(1)}, bf16[384,1024]{1,0:T(8,128)(2,1)}, u32[]{:S(2)}) copy-start(bf16[384,1024]{1,0:T(8,128)(2,1)} %param.8) | copy-start | bytes 2359300
  676.7 65.7 %all-gather.23.cloned.1.call-start = ((), (), s32[]{:S(2)}) async-start(), calls=%async_computation.7 | async-start | bytes 1966080 | tf_op jit(solution)/shard_map/all_gather | solution.py:45
  706.7 5.1 copy-start.5
  706.7 12.9 %slice-start = ((s8[8388608]{0:T(1024)(128)(4,1)}), s8[4194304]{0:T(1024)(128)(4,1)S(1)}, s32[]{:S(2)}) async-start(s8[8388608]{0:T(1024)(128)(4,1)} %bitcast.68), calls=%async_computation.8 | async-start | bytes 8388608
  711.8 7.9 %slice-start.1 = ((s8[8388608]{0:T(1024)(128)(4,1)}), s8[4194304]{0:T(1024)(128)(4,1)S(1)}, s32[]{:S(2)}) async-start(s8[8388608]{0:T(1024)(128)(4,1)} %bitcast.68), calls=%async_computation.9 | async-start | bytes 8388608
  716.0 5.4 collective-permute-start.1
  722.5 24.3 %copy-start = (bf16[384,1024]{1,0:T(8,128)(2,1)S(1)}, bf16[384,1024]{1,0:T(8,128)(2,1)}, u32[]{:S(2)}) copy-start(bf16[384,1024]{1,0:T(8,128)(2,1)} %add_convert_fusion.1) | copy-start | bytes 2359300
Sparse Core Ops, SparseCore 0:
  8.9 31.2 all-gather.8
  41.7 149.6 all-gather.12
  192.9 147.7 all-gather.14
  342.2 147.7 all-gather.10
  491.5 147.7 all-gather.18
  640.7 17.8 all-gather.16
  676.8 29.8 all-gather.20
  722.6 19.7 all-gather.22
where the time goes:
time: 768 us; the launch traced here: 767 us
  waiting for transfers between devices  684 us (89%)
  matrix products  34.6 us (5%)
  blocking collectives  23.1 us (3%)
  between operations  13.8 us (2%)
    all_gather x1, waiting for transfers between devices, local(): lax.all_gather(proj_c, 'sp', axis=1, tiled=True)  151 us
    all_gather x1, waiting for transfers between devices, local(): lax.all_gather(proj_x, 'sp', axis=1, tiled=True)  144 us
    all_gather x1, waiting for transfers between devices, local(): lax.all_gather(proj_out, 'sp', axis=1, tiled=True)  143 us
    all_gather x1, waiting for transfers between devices, local(): lax.all_gather(proj_b, 'sp', axis=1, tiled=True)  143 us
    all_gather x2, waiting for transfers between devices, local(): gathered = lax.all_gather(hidden, 'tp', axis=1, tiled=True)  60.1 us
    all_gather x2, waiting for transfers between devices, local(): all_branch = lax.all_gather(branch, 'tp', axis=1, tiled=True)  39.1 us
  transfers between devices with their start and end apart: 10, of which 8 were waited for; matrix products, arithmetic and copies ran while one was open for 2% of the time, Pallas kernels for 0%

commit v1 on v0

--- a/solution.py
+++ b/solution.py
@@ -23,7 +23,14 @@
         lax.all_gather(proj_out, "sp", axis=1, tiled=True),
     )
     for layer_index in range(LAYERS):
-        gathered = lax.all_gather(hidden, "tp", axis=1, tiled=True)
+        ring = [hidden]
+        for hop in range(3):
+            ring.append(lax.ppermute(ring[-1], "tp", [(dev, (dev + 1) % 4) for dev in range(4)]))
+        gathered = jnp.roll(
+            jnp.concatenate(ring[::-1], axis=1),
+            (lax.axis_index("tp") + 1) * ring[0].shape[1],
+            axis=1,
+        )
         count_rows = gathered.shape[0]
         acc_b = jnp.dot(gathered, whole_b[layer_index], preferred_element_type=jnp.float32)
         acc_c = jnp.dot(gathered, whole_c[layer_index], preferred_element_type=jnp.float32)

time: 768 us -> 745 us (0.970)
  waiting for transfers between devices: 684 us -> 653 us
  other arithmetic: 6.56 us -> 17.4 us
    ppermute x0 -> x6, waiting for transfers between devices: none -> 68.6 us  [local(): lax.ppermute(ring[-1], 'tp', [(dev, (dev + 1) % 4) for dev in range(4)])]
    all_gather x2 -> x0, waiting for transfers between devices: 60.1 us -> none  [local(): gathered = lax.all_gather(hidden, 'tp', axis=1, tiled=True)]
    all_gather x1, waiting for transfers between devices: 151 us -> 111 us  [local(): lax.all_gather(proj_c, 'sp', axis=1, tiled=True)]
    concatenate x0 -> x2, other arithmetic: none -> 11.7 us  [local(): jnp.roll(jnp.concatenate(ring[::-1], axis=1), (lax.axis_index('tp') + 1)...]
  transfers between devices with their start and end apart: 10 -> 14, of which waited for: 8 -> 12; matrix products, arithmetic and copies ran while one was open for 2% -> 3% of each run, Pallas kernels for 0% -> 0%
where the time goes in v1:
time: 745 us; the launch traced here: 744 us
  waiting for transfers between devices  653 us (88%)
  matrix products  31.4 us (4%)
  blocking collectives  23.1 us (3%)
  other arithmetic  17.4 us (2%)
  between operations  13.8 us (2%)
    all_gather x1, waiting for transfers between devices, local(): lax.all_gather(proj_x, 'sp', axis=1, tiled=True)  144 us
    all_gather x1, waiting for transfers between devices, local(): lax.all_gather(proj_out, 'sp', axis=1, tiled=True)  143 us
    all_gather x1, waiting for transfers between devices, local(): lax.all_gather(proj_b, 'sp', axis=1, tiled=True)  143 us
    all_gather x1, waiting for transfers between devices, local(): lax.all_gather(proj_c, 'sp', axis=1, tiled=True)  111 us
    ppermute x6, waiting for transfers between devices, local(): lax.ppermute(ring[-1], 'tp', [(dev, (dev + 1) % 4) for dev in range(4)])  68.6 us
    all_gather x2, waiting for transfers between devices, local(): all_branch = lax.all_gather(branch, 'tp', axis=1, tiled=True)  40.5 us
  transfers between devices with their start and end apart: 14, of which 12 were waited for; matrix products, arithmetic and copies ran while one was open for 3% of the time, Pallas kernels for 0%

profile of v1, /device:TPU:0, one launch (start us, length us, event | category | flops | bytes accessed | tf_op | source)
XLA Modules:
  0.0 744.4 jit_solution(8658051606409236683)
XLA Ops:
  9.9 11.6 %collective-permute-done = bf16[384,1024]{1,0:T(8,128)(2,1)S(1)} collective-permute-done((bf16[384,1024]{1,0:T(8,128)(2,1)S(1)}, bf16[384,1024]{1,0:T(8,128)(2,1)S(1)}, u32[]{:S(2)}, u32[]{:S(2)}) %collective-permute-start) | collective-permute-done | bytes 786464 | tf_op jit(solution)/shard_map/ppermute | solution.py:28
  21.5 11.4 %collective-permute-done.1 = bf16[384,1024]{1,0:T(8,128)(2,1)S(1)} collective-permute-done((bf16[384,1024]{1,0:T(8,128)(2,1)S(1)}, bf16[384,1024]{1,0:T(8,128)(2,1)S(1)}, u32[]{:S(2)}, u32[]{:S(2)}) %collective-permute-start.1) | collective-permute-done | bytes 786464 | tf_op jit(solution)/shard_map/ppermute | solution.py:28
  33.0 11.4 %collective-permute-done.2 = bf16[384,1024]{1,0:T(8,128)(2,1)S(1)} collective-permute-done((bf16[384,1024]{1,0:T(8,128)(2,1)S(1)}, bf16[384,1024]{1,0:T(8,128)(2,1)S(1)}, u32[]{:S(2)}, u32[]{:S(2)}) %collective-permute-start.2) | collective-permute-done | bytes 786464 | tf_op jit(solution)/shard_map/ppermute | solution.py:28
  44.4 6.3 fusion.18
  50.7 110.6 %all-gather.9.cloned.1.call-done = bf16[2,4096,512]{2,1,0:T(8,128)(2,1)} async-done(((bf16[2,1024,512]{2,1,0:T(8,128)(2,1)}), bf16[2,4096,512]{2,1,0:T(8,128)(2,1)}) %all-gather.9.cloned.1.call-update) | async-done | bytes 8388624 | tf_op jit(solution)/shard_map/all_gather | solution.py:21
  161.3 4.9 fusion.25
  166.2 144.5 %all-gather.11.cloned.1.call-done = bf16[2,4096,512]{2,1,0:T(8,128)(2,1)} async-done(((bf16[2,1024,512]{2,1,0:T(8,128)(2,1)}), bf16[2,4096,512]{2,1,0:T(8,128)(2,1)}) %all-gather.11.cloned.1.call-update) | async-done | bytes 8388624 | tf_op jit(solution)/shard_map/all_gather | solution.py:22
  310.7 4.9 fusion.26
  317.1 143.0 %all-gather.7.cloned.1.call-done = bf16[2,4096,512]{2,1,0:T(8,128)(2,1)} async-done(((bf16[2,1024,512]{2,1,0:T(8,128)(2,1)}), bf16[2,4096,512]{2,1,0:T(8,128)(2,1)}) %all-gather.7.cloned.1.call-update) | async-done | bytes 8388624 | tf_op jit(solution)/shard_map/all_gather | solution.py:20
  460.1 4.9 fusion.24
  466.2 143.1 %all-gather.15.cloned.1.call-done = bf16[2,2048,1024]{2,1,0:T(8,128)(2,1)} async-done(((bf16[2,512,1024]{2,1,0:T(8,128)(2,1)}), bf16[2,2048,1024]{2,1,0:T(8,128)(2,1)}) %all-gather.15.cloned.1.call-update) | async-done | bytes 8388624 | tf_op jit(solution)/shard_map/all_gather | solution.py:23
  609.3 19.3 %all-gather.13.cloned.1.call-done = bf16[384,2048]{1,0:T(8,128)(2,1)} async-done(((bf16[384,512]{1,0:T(8,128)(2,1)}), bf16[384,2048]{1,0:T(8,128)(2,1)}) %all-gather.13.cloned.1.call-update) | async-done | bytes 1572880 | tf_op jit(solution)/shard_map/all_gather | solution.py:52
  628.6 4.5 fusion.22
  633.4 5.9 psum.28
  639.7 5.7 psum.29
  645.9 11.4 %collective-permute-done.4 = bf16[384,1024]{1,0:T(8,128)(2,1)S(1)} collective-permute-done((bf16[384,1024]{1,0:T(8,128)(2,1)S(1)}, bf16[384,1024]{1,0:T(8,128)(2,1)S(1)}, u32[]{:S(2)}, u32[]{:S(2)}) %collective-permute-start.4) | collective-permute-done | bytes 786464 | tf_op jit(solution)/shard_map/ppermute | solution.py:28
  657.3 11.4 %collective-permute-done.5 = bf16[384,1024]{1,0:T(8,128)(2,1)S(1)} collective-permute-done((bf16[384,1024]{1,0:T(8,128)(2,1)S(1)}, bf16[384,1024]{1,0:T(8,128)(2,1)S(1)}, u32[]{:S(2)}, u32[]{:S(2)}) %collective-permute-start.5) | collective-permute-done | bytes 786464 | tf_op jit(solution)/shard_map/ppermute | solution.py:28
  668.7 11.4 %collective-permute-done.6 = bf16[384,1024]{1,0:T(8,128)(2,1)S(1)} collective-permute-done((bf16[384,1024]{1,0:T(8,128)(2,1)S(1)}, bf16[384,1024]{1,0:T(8,128)(2,1)S(1)}, u32[]{:S(2)}, u32[]{:S(2)}) %collective-permute-start.6) | collective-permute-done | bytes 786464 | tf_op jit(solution)/shard_map/ppermute | solution.py:28
  680.2 5.4 fusion.11
  685.6 4.2 fusion.29
  698.1 21.2 %all-gather.17.cloned.1.call-done = bf16[384,2048]{1,0:T(8,128)(2,1)} async-done(((bf16[384,512]{1,0:T(8,128)(2,1)}), bf16[384,2048]{1,0:T(8,128)(2,1)}) %all-gather.17.cloned.1.call-update) | async-done | bytes 1572880 | tf_op jit(solution)/shard_map/all_gather | solution.py:52
  719.4 4.5 fusion.23
  724.2 5.9 psum.30
  730.5 5.7 psum.31
  (61 shorter events, 17.6 us)
Async XLA Ops:
  6.5 154.7 %all-gather.9.cloned.1.call-start = ((), (), s32[]{:S(2)}) async-start(), calls=%async_computation.1 | async-start | bytes 10485760 | tf_op jit(solution)/shard_map/all_gather | solution.py:21
  7.3 2.1 copy-start
  7.3 25.7 %copy-start.1 = (f32[2,3,512]{2,0,1:T(2,128)S(1)}, f32[2,3,512]{2,0,1:T(2,128)}, u32[]{:S(2)}) copy-start(f32[2,3,512]{2,0,1:T(2,128)} %param.15) | copy-start | bytes 36868
  7.3 303.4 %all-gather.11.cloned.1.call-start = ((), (), s32[]{:S(2)}) async-start(), calls=%async_computation.2 | async-start | bytes 10485760 | tf_op jit(solution)/shard_map/all_gather | solution.py:22
  8.0 452.1 %all-gather.7.cloned.1.call-start = ((), (), s32[]{:S(2)}) async-start(), calls=%async_computation | async-start | bytes 10485760 | tf_op jit(solution)/shard_map/all_gather | solution.py:20
  8.8 600.6 %all-gather.15.cloned.1.call-start = ((), (), s32[]{:S(2)}) async-start(), calls=%async_computation.4 | async-start | bytes 10485760 | tf_op jit(solution)/shard_map/all_gather | solution.py:23
  9.3 619.3 %all-gather.13.cloned.1.call-start = ((), (), s32[]{:S(2)}) async-start(), calls=%async_computation.3 | async-start | bytes 1966080 | tf_op jit(solution)/shard_map/all_gather | solution.py:52
  9.4 12.1 %collective-permute-start = (bf16[384,1024]{1,0:T(8,128)(2,1)S(1)}, bf16[384,1024]{1,0:T(8,128)(2,1)S(1)}, u32[]{:S(2)}, u32[]{:S(2)}) collective-permute-start(bf16[384,1024]{1,0:T(8,128)(2,1)S(1)} %copy-done), channel_id=1, source_target_pairs={{0,1},{1,2},{2,3},{3,0},{4,5},{5,6},{6,7},{7,4},{8,9},{9,10},{10,1... | collective-permute-start | bytes 2359304 | tf_op jit(solution)/shard_map/ppermute | solution.py:28
  21.5 11.4 %collective-permute-start.1 = (bf16[384,1024]{1,0:T(8,128)(2,1)S(1)}, bf16[384,1024]{1,0:T(8,128)(2,1)S(1)}, u32[]{:S(2)}, u32[]{:S(2)}) collective-permute-start(bf16[384,1024]{1,0:T(8,128)(2,1)S(1)} %collective-permute-done), channel_id=1, source_target_pairs={{0,1},{1,2},{2,3},{3,0},{4,5},{5,6},{6,7},{7,4},{8,9},{9,10},{10,1... | collective-permute-start | bytes 2359304 | tf_op jit(solution)/shard_map/ppermute | solution.py:28
  32.9 11.4 %collective-permute-start.2 = (bf16[384,1024]{1,0:T(8,128)(2,1)S(1)}, bf16[384,1024]{1,0:T(8,128)(2,1)S(1)}, u32[]{:S(2)}, u32[]{:S(2)}) collective-permute-start(bf16[384,1024]{1,0:T(8,128)(2,1)S(1)} %collective-permute-done.1), channel_id=1, source_target_pairs={{0,1},{1,2},{2,3},{3,0},{4,5},{5,6},{6,7},{7,4},{8,9},{9,10},{10,1... | collective-permute-start | bytes 2359304 | tf_op jit(solution)/shard_map/ppermute | solution.py:28
  315.7 150.4 %copy-start.2 = (f32[2,1024]{1,0:T(2,128)S(1)}, f32[2,1024]{1,0:T(2,128)}, u32[]{:S(2)}) copy-start(f32[2,1024]{1,0:T(2,128)} %param.16) | copy-start | bytes 24580
  315.7 150.4 %copy-start.3 = (f32[2,1024]{1,0:T(2,128)S(1)}, f32[2,1024]{1,0:T(2,128)}, u32[]{:S(2)}) copy-start(f32[2,1024]{1,0:T(2,128)} %param.17) | copy-start | bytes 24580
  315.8 149.3 %collective-permute-start.3 = (f32[2,512]{1,0:T(2,128)S(1)}, f32[2,512]{1,0:T(2,128)S(1)}, u32[]{:S(2)}, u32[]{:S(2)}) collective-permute-start(f32[2,512]{1,0:T(2,128)S(1)} %slice.99), channel_id=1, source_target_pairs={{0,4},{4,8},{8,12},{1,5},{5,9},{9,13},{2,6},{6,10},{10,14},{3,7},{... | collective-permute-start | bytes 12296 | tf_op jit(solution)/shard_map/ppermute | solution.py:13
  466.1 253.3 %all-gather.17.cloned.1.call-start = ((), (), s32[]{:S(2)}) async-start(), calls=%async_computation.5 | async-start | bytes 1966080 | tf_op jit(solution)/shard_map/all_gather | solution.py:52
  645.9 11.5 %collective-permute-start.4 = (bf16[384,1024]{1,0:T(8,128)(2,1)S(1)}, bf16[384,1024]{1,0:T(8,128)(2,1)S(1)}, u32[]{:S(2)}, u32[]{:S(2)}) collective-permute-start(bf16[384,1024]{1,0:T(8,128)(2,1)S(1)} %add_convert_fusion.1), channel_id=1, source_target_pairs={{0,1},{1,2},{2,3},{3,0},{4,5},{5,6},{6,7},{7,4},{8,9},{9,10},{10,1... | collective-permute-start | bytes 2359304 | tf_op jit(solution)/shard_map/ppermute | solution.py:28
  657.3 11.4 %collective-permute-start.5 = (bf16[384,1024]{1,0:T(8,128)(2,1)S(1)}, bf16[384,1024]{1,0:T(8,128)(2,1)S(1)}, u32[]{:S(2)}, u32[]{:S(2)}) collective-permute-start(bf16[384,1024]{1,0:T(8,128)(2,1)S(1)} %collective-permute-done.4), channel_id=1, source_target_pairs={{0,1},{1,2},{2,3},{3,0},{4,5},{5,6},{6,7},{7,4},{8,9},{9,10},{10,1... | collective-permute-start | bytes 2359304 | tf_op jit(solution)/shard_map/ppermute | solution.py:28
  668.7 11.4 %collective-permute-start.6 = (bf16[384,1024]{1,0:T(8,128)(2,1)S(1)}, bf16[384,1024]{1,0:T(8,128)(2,1)S(1)}, u32[]{:S(2)}, u32[]{:S(2)}) collective-permute-start(bf16[384,1024]{1,0:T(8,128)(2,1)S(1)} %collective-permute-done.5), channel_id=1, source_target_pairs={{0,1},{1,2},{2,3},{3,0},{4,5},{5,6},{6,7},{7,4},{8,9},{9,10},{10,1... | collective-permute-start | bytes 2359304 | tf_op jit(solution)/shard_map/ppermute | solution.py:28
  680.2 9.6 %slice-start = ((s8[8388608]{0:T(1024)(128)(4,1)}), s8[4194304]{0:T(1024)(128)(4,1)S(1)}, s32[]{:S(2)}) async-start(s8[8388608]{0:T(1024)(128)(4,1)} %bitcast.68), calls=%async_computation.6 | async-start | bytes 8388608
  685.5 4.2 slice-start.1
  685.6 9.7 %slice-start.2 = ((s8[8388608]{0:T(1024)(128)(4,1)}), s8[4194304]{0:T(1024)(128)(4,1)S(1)}, s32[]{:S(2)}) async-start(s8[8388608]{0:T(1024)(128)(4,1)} %bitcast.70), calls=%async_computation.8 | async-start | bytes 8388608
  689.8 5.5 slice-start.3
  691.7 5.4 collective-permute-start.7
Sparse Core Ops, SparseCore 0:
  8.9 152.3 all-gather.8
  162.8 147.7 all-gather.10
  312.2 147.7 all-gather.6
  461.5 147.7 all-gather.14
  610.7 17.8 all-gather.12
  698.3 21.0 all-gather.16
